TPU v7x, 256 devices: a 4x2x16 block of a 4x16x16 slice. The times are simulated.
256 devices in a mesh: grp: 2 (over y), sp: 32 (over z, core), tp: 4 (over x).
Axes of the slice: x: 4, y: 2, z: 16, core: 2. Of those that a mesh axis runs over, the one named last changes fastest.
The devices are a block of a 4x16x16 slice.
Arguments:
- resid_in: bfloat16 [16384, 2048], P(('grp', 'sp', 'tp')), parts along dimension 0, may hold values from -3 to 3
- queries: bfloat16 [16384, 1024], P(('grp', 'sp'), 'tp'), parts along dimension 0, may hold values from -39 to 39
- keys: bfloat16 [16384, 1024], P(('grp', 'sp'), 'tp'), parts along dimension 0, may hold values from -6 to 6
- values: bfloat16 [16384, 1024], P(('grp', 'sp'), 'tp'), parts along dimension 0, may hold values from -12 to 12
- cum_gate: float32 [16384, 16], P('grp', 'tp'), parts along dimension 0, may hold values from -822 to 0, as said below
- w_out: bfloat16 [1024, 2048], replicated, may hold values from -0.1875 to 0.1875
- norm_gain: float32 [2048], replicated, may hold values from 0.1 to 1.9
- w_gate: bfloat16 [2048, 5632], P('sp', 'tp'), may hold values from -0.125 to 0.125
- w_up: bfloat16 [2048, 5632], P('sp', 'tp'), may hold values from -0.125 to 0.125
- w_down: bfloat16 [5632, 2048], P('tp', 'sp'), may hold values from -0.078125 to 0.078125
Outputs:
- resid_out: bfloat16 [16384, 2048], P(('grp', 'sp', 'tp')), parts along dimension 0
There are 2 independent parts, one for each index of `grp`. A program takes and returns all parts, laid end to end along the dimension named above; an argument that names none is the same for every part. Nothing has to cross between parts.
Inputs may be any that keep to these rules, and one draw needn't show every extreme that they name: `cum_gate`: in every head the values never rise from one position to the next, and the first is at most 0.
All inputs are finite; a program needn't handle non-finite values.
Results may differ from a plain program's by a relative error of at most 0.018.
Values may be sent and summed in bfloat16 or wider, within the bound.
A program may use at most 128 MiB of HBM per device.

v0:
```python
import math
import jax
import jax.numpy as jnp
from jax import lax
from jax.sharding import PartitionSpec as P

HEAD_DIM = 64


def sent_together(arrays, axis, dim, along):
    both = jnp.concatenate(arrays, axis=along)
    filled, at, finished = (lax.all_gather(both, axis, axis=dim, tiled=True), 0, [])
    for a in arrays:
        finished.append(lax.slice_in_dim(filled, at, at + a.shape[along], axis=along))
        at += a.shape[along]
    return tuple(finished)


def laid_out(blocks, dim):
    shape = list(blocks.shape[1:])
    shape[dim] *= blocks.shape[0]
    return jnp.moveaxis(blocks, 0, dim).reshape(shape)


def from_everyone(array, axis):
    length = lax.axis_size(axis)
    return lax.all_to_all(
        jnp.broadcast_to(array[None], (length, *array.shape)), axis, 0, 0, tiled=True
    )


def gathered_copies(array, axis, dim):
    return laid_out(from_everyone(array, axis), dim)


def turned_gather(arrays, axis, dims):
    turned = [jnp.moveaxis(a, dim, 0) for a, dim in zip(arrays, dims)]
    both = jnp.concatenate([t.reshape(len(t), -1) for t in turned], axis=1)
    filled, at, finished = (lax.all_gather(both, axis, axis=0, tiled=True), 0, [])
    for t, dim in zip(turned, dims):
        share = filled[:, at : at + t[0].size].reshape(-1, *t.shape[1:])
        finished.append(jnp.moveaxis(share, 0, dim))
        at += t[0].size
    return tuple(finished)


def in_blocks(array, dim, length):
    shape = array.shape
    blocks = array.reshape(*shape[:dim], length, shape[dim] // length, *shape[dim + 1 :])
    return jnp.moveaxis(blocks, dim, 0)


def sum_at_owner(array, axis, dim):
    length = lax.axis_size(axis)
    blocks = lax.all_to_all(in_blocks(array, dim, length), axis, 0, 0, tiled=True)
    return jnp.sum(blocks.astype(jnp.float32), axis=0)


def on_device(resid_in, queries, keys, values, cum_gate, w_out, norm_gain, w_gate, w_up, w_down):
    tok_rows = queries.shape[0]
    local_heads = queries.shape[1] // HEAD_DIM
    scale = HEAD_DIM ** (-0.5)
    offset = lax.axis_index("sp") * tok_rows
    query_heads = queries.reshape(tok_rows, local_heads, HEAD_DIM)
    own_gate = lax.dynamic_slice_in_dim(cum_gate, offset, tok_rows, 0).T
    query_pos = offset + jnp.arange(tok_rows, dtype=jnp.int32)
    last_pos = offset + tok_rows - 1
    initial = (
        jnp.full((local_heads, tok_rows), -1e30, jnp.float32),
        jnp.zeros((local_heads, tok_rows), jnp.float32),
        jnp.zeros((tok_rows, local_heads, HEAD_DIM), jnp.float32),
    )
    key_piece, value_piece = sent_together((keys, values), "sp", 0, 1)
    length = key_piece.shape[0]
    span = math.gcd(length, 512)

    def block(index, state):
        begin = index * span

        def work(inner):
            maxima, totals, summed = inner
            key_block = lax.dynamic_slice_in_dim(key_piece, index * span, span, 0).reshape(
                span, local_heads, HEAD_DIM
            )
            value_block_rows = lax.dynamic_slice_in_dim(value_piece, index * span, span, 0).reshape(
                span, local_heads, HEAD_DIM
            )
            key_gate = lax.dynamic_slice_in_dim(cum_gate, begin, span, 0).T
            scores = (
                jnp.einsum(
                    "qhd,khd->hqk", query_heads, key_block, preferred_element_type=jnp.float32
                )
                * scale
            )
            scores = scores + own_gate[:, :, None] - key_gate[:, None, :]
            key_pos = begin + jnp.arange(span, dtype=jnp.int32)
            mask = (key_pos[None, :] <= query_pos[:, None])[None]
            scores = jnp.where(mask, scores, -1e30)
            new_max = jnp.maximum(maxima, jnp.max(scores, axis=-1))
            weights = jnp.where(mask, jnp.exp(scores - new_max[:, :, None]), 0.0)
            rescale = jnp.exp(maxima - new_max)
            totals = totals * rescale + jnp.sum(weights, axis=-1)
            product = jnp.einsum(
                "hqk,khd->qhd",
                weights.astype(jnp.bfloat16),
                value_block_rows,
                preferred_element_type=jnp.float32,
            )
            summed = summed * rescale.T[:, :, None] + product
            return (new_max, totals, summed)

        return lax.cond(begin <= last_pos, work, lambda inner: inner, state)

    maxima, totals, summed = lax.fori_loop(0, length // span, block, initial)
    attended = (
        (summed / totals.T[:, :, None])
        .reshape(tok_rows, local_heads * HEAD_DIM)
        .astype(jnp.bfloat16)
    )
    head_rows = lax.all_to_all(attended, "tp", split_axis=0, concat_axis=1, tiled=True)
    mixed = jnp.dot(head_rows, w_out, preferred_element_type=jnp.float32)
    resid = resid_in.astype(jnp.float32) + mixed
    normed = resid * lax.rsqrt(jnp.mean(resid * resid, axis=-1, keepdims=True) + 1e-06)
    normed = (normed * norm_gain).astype(jnp.bfloat16)
    all_rows = gathered_copies(normed, "tp", 0)
    full_gate, full_up, full_down = turned_gather((w_gate, w_up, w_down), "sp", (0, 0, 1))
    gate = jnp.dot(all_rows, full_gate, preferred_element_type=jnp.float32)
    up = jnp.dot(all_rows, full_up, preferred_element_type=jnp.float32)
    hidden = (jax.nn.silu(gate) * up).astype(jnp.bfloat16)
    terms = jnp.dot(hidden, full_down, preferred_element_type=jnp.float32)
    back = sum_at_owner(terms.astype(jnp.bfloat16), "tp", 0)
    return (resid + back).astype(jnp.bfloat16)


def solution(mesh):
    return jax.shard_map(
        on_device,
        mesh=mesh,
        in_specs=(
            P(("grp", "sp", "tp"), None),
            P(("grp", "sp"), "tp"),
            P(("grp", "sp"), "tp"),
            P(("grp", "sp"), "tp"),
            P("grp", "tp"),
            P(),
            P(),
            P("sp", "tp"),
            P("sp", "tp"),
            P("tp", "sp"),
        ),
        out_specs=P(("grp", "sp", "tp"), None),
        check_vma=False,
    )
```

profile of v0, /device:TPU:33, one launch (start us, length us, event | category | flops | bytes accessed | tf_op | source)
XLA Modules:
  0.0 264.1 jit_solution(7843677757114892416)
XLA Ops:
  6.6 1.0 copy.16
  7.6 1.0 copy.17
  8.6 0.7 pad_maximum_fusion.1
  9.3 0.1 all-gather.3.cloned.1.call-update
  9.4 0.1 all-gather.5.cloned.1.call-start
  9.5 2.0 pad_maximum_fusion
  11.4 0.1 all-gather.5.cloned.1.call-update
  11.5 0.1 copy.18
  11.6 0.7 dynamic-slice_bitcast_fusion.1
  12.3 106.1 %all-gather.3.cloned.1.call-done = bf16[8192,512]{0,1:T(8,128)(2,1)} async-done(((bf16[256,512]{0,1:T(8,128)(2,1)}), bf16[8192,512]{0,1:T(8,128)(2,1)}) %all-gather.3.cloned.1.call-update) | async-done | bytes 8388624 | tf_op jit(solution)/shard_map/all_gather | solution.py:12
  118.4 5.9 %fusion.36 = (bf16[8192,256]{0,1:T(8,128)(2,1)}, bf16[8192,256]{0,1:T(8,128)(2,1)}) fusion(bf16[8192,512]{0,1:T(8,128)(2,1)} %all-gather.3.cloned.1.call-done), kind=kLoop, calls=%fused_computation.47 | loop fusion | bytes 16777216 | tf_op jit(solution)/shard_map/slice | solution.py:14
  124.4 4.6 %while.18 = (s32[]{:T(128)}, f32[4,256]{1,0:T(4,128)S(1)}, f32[4,256]{1,0:T(4,128)S(1)}, f32[256,4,64]{0,2,1:T(8,128)S(1)}, s32[]{:T(128)}, /*index=5*/bf16[8192...) while((s32[]{:T(128)}, f32[4,256]{1,0:T(4,128)S(1)}, ...), condition=%wide.region_5.6_spmd.clone, body=%wide.region_0.5_spmd.clone.sunk | while | flops 140250880 | bytes 9146775 | solution.py:114
  124.4 3.7 %conditional.3 = ((f32[4,256]{1,0:T(4,128)S(1)}, f32[4,256]{1,0:T(4,128)S(1)}, f32[256,4,64]{0,2,1:T(8,128)S(1)})) conditional(s32[]{:T(128)} %convert_element_type.56, (f32[4,256]{1,0:T(4,128)S(1)}, f32[4,256]{1,0:T(4,128)S(1)}, f32[256,4,64]{0,2,1:T(8,128)S(1)}) %tuple.47, (s32[]{:T(128)}, s32[]{:T(128)}, s32[]{:T(128)}, ...), branch_computations={%region_1.0_spmd, %region_2.4_spmd} | conditional | flops 140250880 | bytes 9145472 | solution.py:112
  124.5 0.7 dynamic-slice_bitcast_fusion
  125.2 0.1 broadcast_compare_fusion
  125.3 1.1 constant_dynamic-slice_fusion
  126.4 0.7 fusion.35
  127.1 0.5 fusion.4
  127.7 0.4 fusion.3
  129.0 0.2 reshape.69
  129.1 0.2 copy.22
  129.3 8.7 %all_to_all.26 = bf16[4,64,256]{2,1,0:T(8,128)(2,1)S(1)} all-to-all(bf16[4,64,256]{2,1,0:T(8,128)(2,1)S(1)} %copy.22), channel_id=1, replica_groups=mesh['grp'=2,'sp'=32,'tp'=4] {'tp'}, dimensions={0} | all-to-all | bytes 262144 | tf_op jit(solution)/shard_map/all_to_all | solution.py:120
  138.0 3.2 %multiply_reduce_fusion = (f32[64]{0:T(128)S(1)}, f32[64,2048]{1,0:T(8,128)S(1)}) fusion(bf16[64,1024]{1,0:T(8,128)(2,1)S(1)} %bitcast.37, bf16[1024,2048]{1,0:T(8,128)(2,1)} %param.19, bf16[64,2048]{1,0:T(8,128)(2,1)S(1)} %copy-done), kind=kOutput, calls=%fused_computation.40 | convolution fusion | flops 268959680 | bytes 5112064 | tf_op jit(solution)/shard_map/dot_general | solution.py:121
  141.3 0.1 multiply_convert_fusion
  141.4 0.1 broadcast_in_dim.46
  141.5 16.0 %all_to_all.27 = bf16[4,64,2048]{2,1,0:T(8,128)(2,1)S(1)} all-to-all(bf16[4,64,2048]{2,1,0:T(8,128)(2,1)S(1)} %broadcast_in_dim.46), channel_id=1, replica_groups=mesh['grp'=2,'sp'=32,'tp'=4] {'tp'}, dimensions={0} | all-to-all | bytes 2097152 | tf_op jit(solution)/shard_map/all_to_all | solution.py:27
  157.5 66.6 %all-gather.5.cloned.1.call-done = bf16[2048,4224]{1,0:T(8,128)(2,1)} async-done(((bf16[64,4224]{1,0:T(8,128)(2,1)}), bf16[2048,4224]{1,0:T(8,128)(2,1)}) %all-gather.5.cloned.1.call-update) | async-done | bytes 17301520 | tf_op jit(solution)/shard_map/all_gather | solution.py:39
  224.1 5.6 %fusion.15 = f32[256,1408]{1,0:T(8,128)} fusion(bf16[256,2048]{1,0:T(8,128)(2,1)S(1)} %bitcast.33, bf16[2048,4224]{1,0:T(8,128)(2,1)} %all-gather.5.cloned.1.call-done), kind=kOutput, calls=%fused_computation.24 | convolution fusion | flops 1476395008 | bytes 8257536 | tf_op jit(solution)/shard_map/dot_general | solution.py:127
  229.7 8.2 %fusion.23 = bf16[256,2048]{1,0:T(8,128)(2,1)S(1)} fusion(bf16[2048,4224]{1,0:T(8,128)(2,1)} %all-gather.5.cloned.1.call-done, bf16[256,2048]{1,0:T(8,128)(2,1)S(1)} %bitcast.34, f32[256,1408]{1,0:T(8,128)} %fusion.15), kind=kOutput, calls=%fused_computation.28 | convolution fusion | flops 2955476992 | bytes 15073280 | tf_op jit(solution)/shard_map/dot_general | solution.py:130
  237.9 18.4 %all_to_all.28 = bf16[4,64,2048]{2,1,0:T(8,128)(2,1)S(1)} all-to-all(bf16[4,64,2048]{2,1,0:T(8,128)(2,1)S(1)} %bitcast.35), channel_id=1, replica_groups=mesh['grp'=2,'sp'=32,'tp'=4] {'tp'}, dimensions={0} | all-to-all | bytes 2097152 | tf_op jit(solution)/shard_map/all_to_all | solution.py:55
  256.3 0.2 convert_reduce_fusion
  256.5 0.8 add_convert_fusion
  (49 shorter events, 0.4 us)
Async XLA Ops:
  6.5 4.9 %copy-start.1 = (bf16[256,256]{1,0:T(8,128)(2,1)S(1)}, bf16[256,256]{1,0:T(8,128)(2,1)}, u32[]{:S(2)}) copy-start(bf16[256,256]{1,0:T(8,128)(2,1)} %param.15) | copy-start | bytes 393220
  6.5 111.8 %all-gather.3.cloned.1.call-start = ((), (), s32[]{:S(2)}) async-start(), calls=%async_computation.3 | async-start | bytes 8650752 | tf_op jit(solution)/shard_map/all_gather | solution.py:12
  9.4 214.7 %all-gather.5.cloned.1.call-start = ((), (), s32[]{:S(2)}) async-start(), calls=%async_computation.4 | async-start | bytes 17842176 | tf_op jit(solution)/shard_map/all_gather | solution.py:39
  124.4 13.7 %copy-start = (bf16[64,2048]{1,0:T(8,128)(2,1)S(1)}, bf16[64,2048]{1,0:T(8,128)(2,1)}, u32[]{:S(2)}) copy-start(bf16[64,2048]{1,0:T(8,128)(2,1)} %param.14) | copy-start | bytes 786436
  138.0 3.3 %copy-start.2 = (f32[2048]{0:T(1024)S(1)}, f32[2048]{0:T(1024)}, u32[]{:S(2)}) copy-start(f32[2048]{0:T(1024)} %param.20) | copy-start | bytes 24580
Sparse Core Ops, SparseCore 0:
  9.5 108.8 all-gather.2
  120.2 103.8 all-gather.4
where the time goes:
time: 265 us; the launch traced here: 264 us
  waiting for transfers between devices  173 us (65%)
  blocking collectives  43.1 us (16%)
  matrix products  18.3 us (7%)
  between operations  13.6 us (5%)
  local copies, waits for them, and re-layouts  11.1 us (4%)
  other arithmetic  4.31 us (2%)
    all_gather x1, waiting for transfers between devices, sent_together(): lax.all_gather(both, axis, axis=dim, tiled=True)  106 us
    all_gather x1, waiting for transfers between devices, turned_gather(): lax.all_gather(both, axis, axis=0, tiled=True)  66.6 us
    all_to_all x1, blocking collectives, sum_at_owner(): lax.all_to_all(in_blocks(array, dim, length), axis, 0, 0, tiled=True)  18.4 us
    all_to_all x1, blocking collectives, from_everyone(): lax.all_to_all(jnp.broadcast_to(array[None], (length, *array.shape)), axi...  16 us
    all_to_all x1, blocking collectives, on_device(): lax.all_to_all(attended, 'tp', split_axis=0, concat_axis=1, tiled=True)  8.67 us
    dot_general x1, matrix products, on_device(): terms = jnp.dot(hidden, full_down, preferred_element_type=jnp.float32)  8.19 us
    slice x1, local copies, waits for them, and re-layouts, sent_together(): lax.slice_in_dim(filled, at, at + a.shape[along], axis=along)  5.93 us
    dot_general x1, matrix products, on_device(): gate = jnp.dot(all_rows, full_gate, preferred_element_type=jnp.float32)  5.59 us
  transfers between devices with their start and end apart: 2, of which 2 were waited for; matrix products, arithmetic and copies ran while one was open for 6% of the time, Pallas kernels for 0%

commit v1 on v0

--- a/solution.py
+++ b/solution.py
@@ -36,7 +36,13 @@
 def turned_gather(arrays, axis, dims):
     turned = [jnp.moveaxis(a, dim, 0) for a, dim in zip(arrays, dims)]
     both = jnp.concatenate([t.reshape(len(t), -1) for t in turned], axis=1)
-    filled, at, finished = (lax.all_gather(both, axis, axis=0, tiled=True), 0, [])
+    filled, at, finished = (
+        jnp.concatenate(
+            lax.all_to_all(jnp.stack([both] * lax.axis_size(axis)), axis, 0, 0), axis=0
+        ),
+        0,
+        [],
+    )
     for t, dim in zip(turned, dims):
         share = filled[:, at : at + t[0].size].reshape(-1, *t.shape[1:])
         finished.append(jnp.moveaxis(share, 0, dim))

time: 265 us -> 1020 us (3.85)
  blocking collectives: 43.1 us -> 840 us
  waiting for transfers between devices: 173 us -> 121 us
    all_to_all x1, blocking collectives: 16 us -> 814 us  [turned_gather(): lax.all_to_all(jnp.stack([both] * lax.axis_size(axis)), axis, 0, 0)]
    all_gather x1 -> x0, waiting for transfers between devices: 66.6 us -> none  [turned_gather(): lax.all_gather(both, axis, axis=0, tiled=True)]
    all_to_all x0 -> x1, waiting for transfers between devices: none -> 13.3 us  [from_everyone(): lax.all_to_all(jnp.broadcast_to(array[None], (length, *array.shape)), axi...]
  transfers between devices with their start and end apart: 2 -> 2, of which waited for: 2 -> 2; matrix products, arithmetic and copies ran while one was open for 6% -> 0% of each run, Pallas kernels for 0% -> 0%
where the time goes in v1:
time: 1020 us
  blocking collectives  840 us (82%)
  waiting for transfers between devices  121 us (12%)
  local copies, waits for them, and re-layouts  20.8 us (2%)
  matrix products  15.6 us (2%)
  between operations  13.6 us (1%)
    all_to_all x1, blocking collectives, turned_gather(): lax.all_to_all(jnp.stack([both] * lax.axis_size(axis)), axis, 0, 0)  814 us
    all_gather x1, waiting for transfers between devices, sent_together(): lax.all_gather(both, axis, axis=dim, tiled=True)  107 us
  transfers between devices with their start and end apart: 2, of which 2 were waited for; matrix products, arithmetic and copies ran while one was open for 0% of the time, Pallas kernels for 0%

profile of v1, /device:TPU:33, one launch (start us, length us, event | category | flops | bytes accessed | tf_op | source)
XLA Modules:
  0.0 1017.1 jit_solution(11812430874341051000)
XLA Ops:
  6.6 1.0 copy.17
  7.6 1.0 copy.16
  8.6 0.7 pad_maximum_fusion.1
  9.3 0.1 all-gather.2.cloned.1.call-update
  9.4 1.0 copy.18
  10.4 0.7 dynamic-slice_bitcast_fusion.1
  11.1 107.3 %all-gather.2.cloned.1.call-done = bf16[8192,512]{0,1:T(8,128)(2,1)} async-done(((bf16[256,512]{0,1:T(8,128)(2,1)}), bf16[8192,512]{0,1:T(8,128)(2,1)}) %all-gather.2.cloned.1.call-update) | async-done | bytes 8388624 | tf_op jit(solution)/shard_map/all_gather | solution.py:12
  118.4 5.9 fusion.36
  124.3 4.6 while.18
  124.3 3.7 conditional.3
  124.3 0.7 dynamic-slice_bitcast_fusion
  125.0 1.1 constant_dynamic-slice_fusion
  126.1 0.1 broadcast_compare_fusion
  126.3 0.7 fusion.35
  127.0 0.4 fusion.3
  127.4 0.5 fusion.4
  128.9 0.2 reshape.75
  129.0 0.2 copy.22
  129.2 8.6 all_to_all.31
  137.9 3.2 multiply_reduce_fusion
  141.1 0.1 multiply_convert_fusion
  141.2 1.1 broadcast_in_dim.46
  142.3 3.6 all-to-all-start.1
  146.0 13.3 %all-to-all-done.1 = bf16[4,64,2048]{2,1,0:T(8,128)(2,1)S(1)} async-done(((bf16[4,64,2048]{2,1,0:T(8,128)(2,1)}), bf16[4,64,2048]{2,1,0:T(8,128)(2,1)S(1)}, u32[]{:S(2)}, u32[]{:S(2)}) %all-to-all-start.1) | async-done | bytes 1048608 | tf_op jit(solution)/shard_map/all_to_all | solution.py:27
  159.3 2.1 stack.2
  161.4 813.8 %all_to_all.32 = bf16[32,64,4224]{2,1,0:T(8,128)(2,1)S(1)} all-to-all(bf16[32,64,4224]{2,1,0:T(8,128)(2,1)S(1)} %stack.2), channel_id=1, replica_groups=mesh['grp'=2,'sp'=32,'tp'=4] {'sp'}, dimensions={0} | all-to-all | bytes 34603008 | tf_op jit(solution)/shard_map/all_to_all | solution.py:41
  975.1 5.9 copy-done
  981.0 3.0 fusion.15
  984.0 8.2 fusion.23
  992.2 17.1 %all_to_all.33 = bf16[4,64,2048]{2,1,0:T(8,128)(2,1)S(1)} all-to-all(bf16[4,64,2048]{2,1,0:T(8,128)(2,1)S(1)} %bitcast.38), channel_id=1, replica_groups=mesh['grp'=2,'sp'=32,'tp'=4] {'tp'}, dimensions={0} | all-to-all | bytes 2097152 | tf_op jit(solution)/shard_map/all_to_all | solution.py:61
  1009.3 0.2 convert_reduce_fusion
  1009.5 0.8 add_convert_fusion
  (55 shorter events, 0.4 us)
Async XLA Ops:
  6.5 111.8 %all-gather.2.cloned.1.call-start = ((), (), s32[]{:S(2)}) async-start(), calls=%async_computation.4 | async-start | bytes 8650752 | tf_op jit(solution)/shard_map/all_gather | solution.py:12
  124.2 13.6 %copy-start.1 = (bf16[64,2048]{1,0:T(8,128)(2,1)S(1)}, bf16[64,2048]{1,0:T(8,128)(2,1)}, u32[]{:S(2)}) copy-start(bf16[64,2048]{1,0:T(8,128)(2,1)} %param.14) | copy-start | bytes 786436
  137.8 3.2 copy-start.5
  141.0 4.9 copy-start.2
  141.1 4.9 copy-start.3
  141.1 4.9 copy-start.4
  142.3 17.0 %all-to-all-start.1 = ((bf16[4,64,2048]{2,1,0:T(8,128)(2,1)}), bf16[4,64,2048]{2,1,0:T(8,128)(2,1)S(1)}, u32[]{:S(2)}, u32[]{:S(2)}) async-start(bf16[4,64,2048]{2,1,0:T(8,128)(2,1)} %broadcast_in_dim.46), calls=%async_computation.1 | async-start | bytes 2097152 | tf_op jit(solution)/shard_map/all_to_all | solution.py:27
  975.1 5.9 copy-start
Sparse Core Ops, SparseCore 0:
  9.5 108.8 all-gather.1
